TPU v7x, 1024 devices: a whole 4x4x32 slice. The times are simulated.
1024 devices in a mesh: row: 64 (over z, core), col: 16 (over y, x).
Axes of the slice: x: 4, y: 4, z: 32, core: 2. Of those that a mesh axis runs over, the one named last changes fastest.
Arguments:
- tokens: bfloat16 [32768, 2048], P('row'), may hold values from -6 to 6
- out_weight: bfloat16 [2048, 2048], P(None, 'col'), may hold values from -0.125 to 0.125
Outputs:
- mixed: bfloat16 [32768, 2048], P('row', 'col')
All inputs are finite; a program needn't handle non-finite values.
Results may differ from a plain program's by a relative error of at most 0.001.
Values may be sent and summed in bfloat16 or wider, within the bound.
A program may use at most 64 MiB of HBM per device.

v0:
```python
import functools
import math

import jax
import jax.numpy as jnp
import numpy as np
from jax import lax
from jax.experimental import pallas as pl
from jax.experimental.pallas import tpu as pltpu
from jax.sharding import PartitionSpec as P

GROUPS = 4
GROUP_DIM = 512
MESH_ID = pl.DeviceIdType.MESH
BF16 = jnp.bfloat16
F32 = jnp.float32

FLOOR = 2.0**-6
LIMIT = 34800.0
SHIFT = 87.0
GAIN = 175.0 / math.log1p(LIMIT / FLOOR)


def split_table(table):
    hi = table.astype(np.float32).astype(jnp.bfloat16)
    lo = (table - hi.astype(np.float64)).astype(np.float32).astype(jnp.bfloat16)
    return hi, lo


def make_tables(row_count, seg_rows):
    length = row_count * seg_rows
    idx = np.arange(seg_rows)
    phase = (idx[:, None] * idx[None, :]) % seg_rows * (2 * np.pi / seg_rows)
    cos_hi, cos_lo = split_table(np.cos(phase))
    sin_hi, sin_lo = split_table(np.sin(phase))
    seg_table = np.concatenate([cos_hi, cos_lo, sin_hi, sin_lo], axis=0)
    row = np.arange(row_count)
    phase = (row[:, None] * row[None, :]) % row_count * (2 * np.pi / row_count)
    cos, sin = np.cos(phase), np.sin(phase)
    row_hi, row_lo = split_table(np.block([[cos, sin], [-sin, cos]]))
    row_table = np.concatenate([row_hi, row_lo], axis=0)
    phase = (row[:, None] * idx[None, :]) % length * (2 * np.pi / length)
    scaling = 1.0 / math.sqrt(length * GROUP_DIM)
    twist = np.concatenate([np.cos(phase), np.sin(phase)], axis=0) * scaling
    perm = np.zeros((256, 256), np.float32)
    for part in range(2):
        for chan in range(2):
            perm[4 * row + 2 * part + chan, part * 128 + chan * 64 + row] = 1.0
    return seg_table, row_table, twist.astype(np.float32), perm.astype(jnp.bfloat16)


def dot(a, b):
    return jnp.dot(a, b, preferred_element_type=F32)


def dot_t(a, b):
    return lax.dot_general(a, b, (((1,), (1,)), ((), ())), preferred_element_type=F32)


def halves(value):
    hi = value.astype(BF16)
    return hi, (value - hi.astype(F32)).astype(BF16)


def encode(value):
    size = jnp.exp(GAIN * jnp.log(1.0 + jnp.abs(value) * (1.0 / FLOOR)) - SHIFT)
    return jnp.where(value < 0.0, -size, size)


def decode(coded):
    size = FLOOR * (jnp.exp((jnp.log(jnp.abs(coded)) + SHIFT) * (1.0 / GAIN)) - 1.0)
    return jnp.where(coded < 0.0, -size, size)


def kernel(
    rows,
    x_hbm, w_hbm, seg_hbm, row_hbm, twist_hbm, perm_hbm, out_ref,
    x, w, seg, row_tab, twist, perm, fold, spread, send1, recv1, send2, recv2, spread2,
    load_sem, send_sem, recv_sem,
):
    me = lax.axis_index("row")
    col = lax.axis_index("col")
    chips = rows // 2
    chip = me // 2
    core = lax.rem(me, 2)

    loads = []
    for i, (src, dst) in enumerate(
        [(w_hbm, w), (seg_hbm, seg), (x_hbm, x), (perm_hbm, perm), (row_hbm, row_tab), (twist_hbm, twist)]
    ):
        load = pltpu.make_async_copy(src, dst, load_sem.at[i])
        load.start()
        loads.append(load)

    barrier = pltpu.get_barrier_semaphore()

    def greet(i, carry):
        pl.semaphore_signal(
            barrier, inc=1, device_id=(lax.rem(me + i, rows), col), device_id_type=MESH_ID
        )
        return carry

    lax.fori_loop(1, rows, greet, 0)

    def exchange(src, dst, which):
        def one(step, target_core):
            target = lax.rem(chip + step + chips, chips) * 2 + target_core
            pltpu.make_async_remote_copy(
                src_ref=src.at[target],
                dst_ref=dst.at[me],
                send_sem=send_sem.at[which],
                recv_sem=recv_sem.at[which],
                device_id=(target, col),
                device_id_type=MESH_ID,
            ).start()

        half = chips // 2
        one(half, core)
        one(half, 1 - core)

        def ring(i, carry):
            hop = half - 1 - i
            one(hop, core)
            one(-hop, core)
            one(hop, 1 - core)
            one(-hop, 1 - core)
            return carry

        lax.fori_loop(0, half - 1, ring, 0)
        one(0, 1 - core)
        dst[pl.ds(me, 1)] = src[pl.ds(me, 1)]

    def arrived(dst, which):
        part = dst.at[pl.ds(0, rows - 1)]
        pltpu.make_async_copy(part, part, recv_sem.at[which]).wait()

    def departed(src, which):
        part = src.at[pl.ds(0, rows - 1)]
        pltpu.make_async_copy(part, part, send_sem.at[which]).wait()

    loads[0].wait()
    loads[1].wait()
    wide = jnp.concatenate([w[g * 512 : (g + 1) * 512, :] for g in range(GROUPS)], axis=1)
    for part in range(2):
        sign = 1.0 - 2.0 * part
        base = part * 1024
        folded = (dot(seg[base : base + 512, :], wide) + dot(seg[base + 512 : base + 1024, :], wide)) * sign
        hi, lo = halves(folded)
        for g in range(GROUPS):
            fold[g * 512 : (g + 1) * 512, part * 128 : (part + 1) * 128] = hi[:, g * 128 : (g + 1) * 128]
            fold[g * 512 : (g + 1) * 512, 256 + part * 128 : 256 + (part + 1) * 128] = lo[:, g * 128 : (g + 1) * 128]

    loads[2].wait()
    loads[3].wait()
    both = dot(x[...], fold[...])
    coded = encode(both[:, :256] + both[:, 256:]).astype(BF16)
    for q in range(4):
        turned = dot_t(perm[...], coded[q * 128 : (q + 1) * 128, :])
        spread[pl.ds(q, 256, stride=4), :] = turned
    send1[...] = spread[...].astype(BF16).reshape(rows, 16, 128)

    pl.semaphore_wait(barrier, rows - 1)
    exchange(send1, recv1, 0)
    loads[4].wait()
    loads[5].wait()
    arrived(recv1, 0)

    spread[...] = decode(recv1[...].reshape(rows * 16, 128).astype(F32))
    parts = []
    for part in range(2):
        parts.append(
            jnp.concatenate(
                [spread[pl.ds(part * 8 + u, rows, stride=16), :] for u in range(8)], axis=1
            )
        )
    hi, lo = halves(jnp.concatenate(parts, axis=0))
    first = dot(row_tab[:128, :], hi) + dot(row_tab[:128, :], lo) + dot(row_tab[128:, :], hi)
    tc = twist[:rows, :]
    ts = twist[rows:, :]
    real, imag = [], []
    for c in range(2):
        re = first[:rows, c * 512 : (c + 1) * 512]
        im = first[rows:, c * 512 : (c + 1) * 512]
        real.append(tc * re + ts * im)
        imag.append(tc * im - ts * re)
    re_hi, re_lo = halves(jnp.concatenate(real, axis=0))
    im_hi, im_lo = halves(jnp.concatenate(imag, axis=0))
    res = dot_t(seg[0:512, :], re_hi) + dot_t(seg[0:512, :], re_lo) + dot_t(seg[512:1024, :], re_hi)
    res = res + dot_t(seg[1024:1536, :], im_hi) + dot_t(seg[1024:1536, :], im_lo) + dot_t(seg[1536:2048, :], im_hi)
    send2[...] = res.reshape(rows, 8, 128).astype(BF16)
    exchange(send2, recv2, 1)
    arrived(recv2, 1)

    spread2[...] = recv2[...].astype(F32).reshape(rows * 8, 128)
    low = lax.broadcasted_iota(jnp.int32, (rows, 128), 1) < 64
    for pair in range(4):
        even = spread2[pl.ds(2 * pair, rows, stride=8), :]
        odd = spread2[pl.ds(2 * pair + 1, rows, stride=8), :]
        top = jnp.where(low, even, pltpu.roll(odd, 64, 1))
        bottom = jnp.where(low, pltpu.roll(even, 64, 1), odd)
        turned = jnp.concatenate([top, bottom], axis=0).T
        out_ref[pair * 128 : (pair + 1) * 128, :] = turned.astype(BF16)
    departed(send1, 0)
    departed(send2, 1)


def body(tokens, out_weight):
    rows = lax.axis_size("row")
    seg_rows = tokens.shape[0]
    tables = [jnp.asarray(t) for t in make_tables(rows, seg_rows)]
    operands = [tokens, out_weight] + tables
    scratch = [pltpu.VMEM(a.shape, a.dtype) for a in operands]
    scratch += [
        pltpu.VMEM((2048, 512), BF16),
        pltpu.VMEM((rows * 16, 128), F32),
        pltpu.VMEM((rows, 16, 128), BF16),
        pltpu.VMEM((rows, 16, 128), BF16),
        pltpu.VMEM((rows, 8, 128), BF16),
        pltpu.VMEM((rows, 8, 128), BF16),
        pltpu.VMEM((rows * 8, 128), F32),
        pltpu.SemaphoreType.DMA((6,)),
        pltpu.SemaphoreType.DMA((2,)),
        pltpu.SemaphoreType.DMA((2,)),
    ]
    return pl.pallas_call(
        functools.partial(kernel, rows),
        out_shape=jax.ShapeDtypeStruct((seg_rows, out_weight.shape[1]), BF16),
        in_specs=[pl.BlockSpec(memory_space=pl.ANY)] * len(operands),
        out_specs=pl.BlockSpec(memory_space=pltpu.VMEM),
        scratch_shapes=scratch,
        compiler_params=pltpu.CompilerParams(
            collective_id=0, has_side_effects=True, vmem_limit_bytes=60 * 1024 * 1024
        ),
        name="mix",
    )(*operands)


def solution(mesh):
    placed = (P("row", None), P(None, "col"))
    return jax.shard_map(
        body, mesh=mesh, in_specs=placed, out_specs=P("row", "col"), check_vma=False
    )
```

profile of v0, /device:TPU:1, one launch (start us, length us, event | category | flops | bytes accessed | tf_op | source)
XLA Modules:
  0.0 75.2 jit_solution(2609587242989012591)
XLA Ops:
  0.0 73.6 %mix.1 = bf16[512,128]{1,0:T(8,128)(2,1)} custom-call(bf16[512,2048]{1,0:T(8,128)(2,1)} %x_hbm.1, bf16[2048,128]{1,0:T(8,128)(2,1)} %w_hbm.1, bf16[2048,512]{1,0:T(8,128)(2,1)} %constant.8.clone.seg_hbm, bf16[256,128]{1,0:T(8,128)(2,1)} %constant.9.clone.row_hbm, f32[128,512]{1,0:T(8,128)} %constant.10.clone.twist_hbm, bf16[256,256]{1,0:T(8,128)(2,1)} %constant.11.clone.perm_hbm), custom_call_target="tpu_custom_call" | custom-call | tf_op jit(solution)/shard_map/mix/pallas_call | solution.py:225
  73.6 1.6 %copy.8 = bf16[512,128]{1,0:T(8,128)(2,1)} copy(bf16[512,128]{1,0:T(8,128)(2,1)} %mix.1) | data formatting | bytes 262144
where the time goes:
time: 75.3 us; the launch traced here: 75.2 us
  Pallas kernels  73.6 us (98%)
  local copies, waits for them, and re-layouts  1.57 us (2%)
    pallas_call x1, Pallas kernels, body(): pl.pallas_call(functools.partial(kernel, rows), out_shape=jax.ShapeDtypeS...  73.6 us
    unnamed x1, local copies, waits for them, and re-layouts  1.57 us

commit v1 on v0

v1 whole, which is shorter than its diff:
```python
import functools
import math

import jax
import jax.numpy as jnp
import numpy as np
from jax import lax
from jax.experimental import pallas as pl
from jax.experimental.pallas import tpu as pltpu
from jax.sharding import PartitionSpec as P

GROUPS = 4
GROUP_DIM = 512
MESH_ID = pl.DeviceIdType.MESH
BF16 = jnp.bfloat16
F32 = jnp.float32

FLOOR = 2.0**-6
LIMIT = 34800.0
SHIFT = 87.0
GAIN = 175.0 / math.log1p(LIMIT / FLOOR)


EARLY = ((8, 1),)
LATE = ((16, 9),)


def split_table(table):
    hi = table.astype(np.float32).astype(jnp.bfloat16)
    lo = (table - hi.astype(np.float64)).astype(np.float32).astype(jnp.bfloat16)
    return hi, lo


def make_tables(row_count, seg_rows):
    length = row_count * seg_rows
    idx = np.arange(seg_rows)
    phase = (idx[:, None] * idx[None, :]) % seg_rows * (2 * np.pi / seg_rows)
    cos_hi, cos_lo = split_table(np.cos(phase))
    sin_hi, sin_lo = split_table(np.sin(phase))
    row = np.arange(row_count)
    phase = (row[:, None] * row[None, :]) % row_count * (2 * np.pi / row_count)
    cos, sin = np.cos(phase), np.sin(phase)
    row_hi, row_lo = split_table(np.block([[cos, sin], [-sin, cos]]))
    phase = (row[:, None] * idx[None, :]) % length * (2 * np.pi / length)
    scaling = 1.0 / math.sqrt(length * GROUP_DIM)
    twist_hi, twist_lo = split_table(np.concatenate([np.cos(phase), np.sin(phase)], axis=0) * scaling)
    mixed = np.zeros((512, 512), jnp.bfloat16)
    for part in range(2):
        for chan in range(2):
            own = 8 * (row // 2) + 4 * (row % 2) + 2 * part + chan
            swapped = 8 * (row // 2) + 4 * (1 - row % 2) + 2 * part + chan
            source = part * 128 + chan * 64 + row
            mixed[own, source] = 1.0
            mixed[256 + swapped, source] = 1.0
    mixed[:, 256:384] = np.concatenate([row_hi, row_lo, row_hi, row_lo], axis=0)
    return np.concatenate([cos_hi, cos_lo, sin_hi, sin_lo, twist_hi, twist_lo, mixed], axis=0)


def dot(a, b):
    return jnp.dot(a, b, preferred_element_type=F32)


def dot_t(a, b):
    return lax.dot_general(a, b, (((1,), (1,)), ((), ())), preferred_element_type=F32)


def halves(value):
    hi = value.astype(BF16)
    return hi, (value - hi.astype(F32)).astype(BF16)


def encode(value):
    size = jnp.exp(GAIN * jnp.log(1.0 + jnp.abs(value) * (1.0 / FLOOR)) - SHIFT)
    return jnp.where(value < 0.0, -size, size)


def decode(coded):
    size = FLOOR * (jnp.exp((jnp.log(jnp.abs(coded)) + SHIFT) * (1.0 / GAIN)) - 1.0)
    return jnp.where(coded < 0.0, -size, size)


def kernel(
    rows,
    x_hbm, w_hbm, tab_hbm, out_ref,
    x, w, tab, fold, spread, send1, recv1, send2, recv2, spread2,
    load_sem, send_sem, recv_sem, word_sem,
):
    me = lax.axis_index("row")
    col = lax.axis_index("col")
    chips = rows // 2
    chip = me // 2
    core = lax.rem(me, 2)

    loads = []
    for i, (src, dst) in enumerate(
        [
            (w_hbm, w),
            (tab_hbm.at[0:1024], tab.at[0:1024]),
            (tab_hbm.at[1024:2048], tab.at[1024:2048]),
            (x_hbm, x),
            (tab_hbm.at[2048:2816], tab.at[2048:2816]),
        ]
    ):
        load = pltpu.make_async_copy(src, dst, load_sem.at[i])
        load.start()
        loads.append(load)

    barrier = pltpu.get_barrier_semaphore()
    reach = chips // 4

    def place(step, target_core):
        return lax.rem(chip + step + chips, chips) * 2 + target_core

    def signal(sem, step, target_core):
        pl.semaphore_signal(
            sem, inc=1, device_id=(place(step, target_core), col), device_id_type=MESH_ID
        )

    signal(barrier, 0, 1 - core)

    def greet(i, carry):
        for step in (reach - i, i - reach):
            signal(barrier, step, core)
            signal(barrier, step, 1 - core)
        return carry

    lax.fori_loop(0, reach, greet, 0)

    def known_near():
        pl.semaphore_wait(barrier, 4 * reach + 1)
        signal(word_sem, reach, core)
        signal(word_sem, -reach, core)

    def known_all():
        pl.semaphore_wait(word_sem, 2)

    def send(src, dst, which, step, target_core):
        target_chip = lax.rem(chip + step + chips, chips)
        pltpu.make_async_remote_copy(
            src_ref=src.at[target_chip, target_core],
            dst_ref=dst.at[me],
            send_sem=send_sem.at[which],
            recv_sem=recv_sem.at[which],
            device_id=(target_chip * 2 + target_core, col),
            device_id_type=MESH_ID,
        ).start()

    def send_ring(src, dst, which, far, near):
        if far == chips // 2:
            send(src, dst, which, far, core)
            send(src, dst, which, far, 1 - core)
            far -= 1

        def ring(i, carry):
            hop = far - i
            for target_core in (core, 1 - core):
                send(src, dst, which, hop, target_core)
                send(src, dst, which, -hop, target_core)
            return carry

        lax.fori_loop(0, far - near + 1, ring, 0)

    def keep_own(src, dst):
        dst[pl.ds(me, 1)] = src[pl.ds(chip, 1), pl.ds(core, 1)][0]

    def arrived(dst, which):
        part = dst.at[pl.ds(0, rows - 1)]
        pltpu.make_async_copy(part, part, recv_sem.at[which]).wait()

    def departed(dst, which):
        part = dst.at[pl.ds(0, rows - 1)]
        pltpu.make_async_copy(part, part, send_sem.at[which]).wait()

    loads[0].wait()
    wide = jnp.concatenate([w[g * 512 : (g + 1) * 512, :] for g in range(GROUPS)], axis=1)
    for part in range(2):
        loads[1 + part].wait()
        base = part * 1024
        folded = dot(tab[base : base + 512, :], wide) + dot(tab[base + 512 : base + 1024, :], wide)
        hi, lo = halves(-folded if part else folded)
        for g in range(GROUPS):
            fold[g * 512 : (g + 1) * 512, part * 128 : (part + 1) * 128] = hi[:, g * 128 : (g + 1) * 128]
            fold[g * 512 : (g + 1) * 512, 256 + part * 128 : 256 + (part + 1) * 128] = lo[:, g * 128 : (g + 1) * 128]

    loads[3].wait()
    both = dot(x[...], fold[...])
    coded = encode(both[:, :256] + both[:, 256:]).astype(BF16)
    loads[4].wait()
    own = dot_t(tab[2304:2560, 0:256], coded).reshape(rows // 2, 8, 512)
    swapped = dot_t(tab[2560:2816, 0:256], coded).reshape(rows // 2, 8, 512)
    upper = lax.broadcasted_iota(jnp.int32, (rows // 2, 8, 128), 1) < 4
    for parity, (one, two) in enumerate(((own, swapped), (swapped, own))):
        for half in range(2):
            lanes = half * 256
            block = jnp.where(upper, one[:, :, lanes : lanes + 128], two[:, :, lanes + 128 : lanes + 256])
            send1[:, parity, half * 8 : (half + 1) * 8, :] = block.astype(BF16)

    known_near()
    for far, near in EARLY:
        send_ring(send1, recv1, 0, far, near)
    known_all()
    for far, near in LATE:
        send_ring(send1, recv1, 0, far, near)
    send(send1, recv1, 0, 0, 1 - core)
    keep_own(send1, recv1)
    arrived(recv1, 0)

    spread[...] = decode(recv1[...].reshape(rows * 16, 128).astype(F32))
    parts = []
    for part in range(2):
        parts.append(
            jnp.concatenate(
                [
                    spread[pl.ds(4 * q + 2 * part + c, rows, stride=16), :]
                    for c in range(2)
                    for q in range(4)
                ],
                axis=1,
            )
        )
    hi, lo = halves(jnp.concatenate(parts, axis=0))
    row_hi = tab[2304:2432, 256:384]
    first = dot(row_hi, hi) + dot(row_hi, lo) + dot(tab[2432:2560, 256:384], hi)
    twist = tab[2048:2176, :].astype(F32) + tab[2176:2304, :].astype(F32)
    tc = twist[:rows, :]
    ts = twist[rows:, :]
    real, imag = [], []
    for c in range(2):
        re = first[:rows, c * 512 : (c + 1) * 512]
        im = first[rows:, c * 512 : (c + 1) * 512]
        real.append(tc * re + ts * im)
        imag.append(tc * im - ts * re)
    re_hi, re_lo = halves(jnp.concatenate(real, axis=0))
    im_hi, im_lo = halves(jnp.concatenate(imag, axis=0))
    res = dot_t(tab[0:512, :], re_hi) + dot_t(tab[0:512, :], re_lo) + dot_t(tab[512:1024, :], re_hi)
    res = res + dot_t(tab[1024:1536, :], im_hi) + dot_t(tab[1024:1536, :], im_lo) + dot_t(tab[1536:2048, :], im_hi)
    send2[...] = res.reshape(rows // 2, 2, 8, 128).astype(BF16)
    send_ring(send2, recv2, 1, 16, 1)
    send(send2, recv2, 1, 0, 1 - core)
    keep_own(send2, recv2)
    arrived(recv2, 1)

    spread2[...] = recv2[...].astype(F32).reshape(rows * 8, 128)
    low = lax.broadcasted_iota(jnp.int32, (rows, 128), 1) < 64
    for pair in range(4):
        even = spread2[pl.ds(2 * pair, rows, stride=8), :]
        odd = spread2[pl.ds(2 * pair + 1, rows, stride=8), :]
        top = jnp.where(low, even, pltpu.roll(odd, 64, 1))
        bottom = jnp.where(low, pltpu.roll(even, 64, 1), odd)
        turned = jnp.concatenate([top, bottom], axis=0).T
        out_ref[pair * 128 : (pair + 1) * 128, :] = turned.astype(BF16)
    departed(recv1, 0)
    departed(recv2, 1)


def body(tokens, out_weight):
    rows = lax.axis_size("row")
    seg_rows = tokens.shape[0]
    operands = [tokens, out_weight, jnp.asarray(make_tables(rows, seg_rows))]
    scratch = [pltpu.VMEM(a.shape, a.dtype) for a in operands]
    scratch += [
        pltpu.VMEM((2048, 512), BF16),
        pltpu.VMEM((rows * 16, 128), F32),
        pltpu.VMEM((rows // 2, 2, 16, 128), BF16),
        pltpu.VMEM((rows, 16, 128), BF16),
        pltpu.VMEM((rows // 2, 2, 8, 128), BF16),
        pltpu.VMEM((rows, 8, 128), BF16),
        pltpu.VMEM((rows * 8, 128), F32),
        pltpu.SemaphoreType.DMA((5,)),
        pltpu.SemaphoreType.DMA((2,)),
        pltpu.SemaphoreType.DMA((2,)),
        pltpu.SemaphoreType.REGULAR,
    ]
    return pl.pallas_call(
        functools.partial(kernel, rows),
        out_shape=jax.ShapeDtypeStruct((seg_rows, out_weight.shape[1]), BF16),
        in_specs=[pl.BlockSpec(memory_space=pl.ANY)] * len(operands),
        out_specs=pl.BlockSpec(memory_space=pltpu.VMEM),
        scratch_shapes=scratch,
        compiler_params=pltpu.CompilerParams(
            collective_id=0, has_side_effects=True, vmem_limit_bytes=54848 * 1024
        ),
        name="mix",
    )(*operands)


def solution(mesh):
    placed = (P("row", None), P(None, "col"))
    return jax.shard_map(
        body, mesh=mesh, in_specs=placed, out_specs=P("row", "col"), check_vma=False
    )
```

time: 75.3 us -> 71.7 us (0.952)
  Pallas kernels: 73.6 us -> 70.9 us
  local copies, waits for them, and re-layouts: 1.57 us -> 0.66 us
    pallas_call x1, Pallas kernels: 73.6 us -> 70.9 us  [body(): pl.pallas_call(functools.partial(kernel, rows), out_shape=jax.ShapeDtypeS...]
    unnamed x1, local copies, waits for them, and re-layouts: 1.57 us -> 0.66 us
where the time goes in v1:
time: 71.7 us; the launch traced here: 71.5 us
  Pallas kernels  70.9 us (99%)
    pallas_call x1, Pallas kernels, body(): pl.pallas_call(functools.partial(kernel, rows), out_shape=jax.ShapeDtypeS...  70.9 us

profile of v1, /device:TPU:1, one launch (start us, length us, event | category | flops | bytes accessed | tf_op | source)
XLA Modules:
  0.0 71.5 jit_solution(1457263255102473197)
XLA Ops:
  0.0 70.9 %mix.1 = bf16[512,128]{1,0:T(8,128)(2,1)S(1)} custom-call(bf16[512,2048]{1,0:T(8,128)(2,1)} %x_hbm.1, bf16[2048,128]{1,0:T(8,128)(2,1)} %w_hbm.1, bf16[2816,512]{1,0:T(8,128)(2,1)} %constant.2.clone.tab_hbm), custom_call_target="tpu_custom_call" | custom-call | tf_op jit(solution)/shard_map/mix/pallas_call | solution.py:274
  70.9 0.7 copy.5

commit v2 on v1

--- a/solution.py
+++ b/solution.py
@@ -19,10 +19,6 @@
 LIMIT = 34800.0
 SHIFT = 87.0
 GAIN = 175.0 / math.log1p(LIMIT / FLOOR)
-
-
-EARLY = ((8, 1),)
-LATE = ((16, 9),)
 
 
 def split_table(table):
@@ -44,15 +40,11 @@
     phase = (row[:, None] * idx[None, :]) % length * (2 * np.pi / length)
     scaling = 1.0 / math.sqrt(length * GROUP_DIM)
     twist_hi, twist_lo = split_table(np.concatenate([np.cos(phase), np.sin(phase)], axis=0) * scaling)
-    mixed = np.zeros((512, 512), jnp.bfloat16)
+    mixed = np.zeros((256, 512), jnp.bfloat16)
     for part in range(2):
         for chan in range(2):
-            own = 8 * (row // 2) + 4 * (row % 2) + 2 * part + chan
-            swapped = 8 * (row // 2) + 4 * (1 - row % 2) + 2 * part + chan
-            source = part * 128 + chan * 64 + row
-            mixed[own, source] = 1.0
-            mixed[256 + swapped, source] = 1.0
-    mixed[:, 256:384] = np.concatenate([row_hi, row_lo, row_hi, row_lo], axis=0)
+            mixed[128 * chan + 2 * row + part, part * 128 + chan * 64 + row] = 1.0
+    mixed[:, 256:384] = np.concatenate([row_hi, row_lo], axis=0)
     return np.concatenate([cos_hi, cos_lo, sin_hi, sin_lo, twist_hi, twist_lo, mixed], axis=0)
 
 
@@ -98,7 +90,7 @@
             (tab_hbm.at[0:1024], tab.at[0:1024]),
             (tab_hbm.at[1024:2048], tab.at[1024:2048]),
             (x_hbm, x),
-            (tab_hbm.at[2048:2816], tab.at[2048:2816]),
+            (tab_hbm.at[2048:2560], tab.at[2048:2560]),
         ]
     ):
         load = pltpu.make_async_copy(src, dst, load_sem.at[i])
@@ -160,8 +152,8 @@
 
         lax.fori_loop(0, far - near + 1, ring, 0)
 
-    def keep_own(src, dst):
-        dst[pl.ds(me, 1)] = src[pl.ds(chip, 1), pl.ds(core, 1)][0]
+    def keep_own(src, dst, c):
+        dst[c, pl.ds(me, 1)] = src[c, pl.ds(chip, 1), pl.ds(core, 1)][0]
 
     def arrived(dst, which):
         part = dst.at[pl.ds(0, rows - 1)]
@@ -186,71 +178,65 @@
     both = dot(x[...], fold[...])
     coded = encode(both[:, :256] + both[:, 256:]).astype(BF16)
     loads[4].wait()
-    own = dot_t(tab[2304:2560, 0:256], coded).reshape(rows // 2, 8, 512)
-    swapped = dot_t(tab[2560:2816, 0:256], coded).reshape(rows // 2, 8, 512)
-    upper = lax.broadcasted_iota(jnp.int32, (rows // 2, 8, 128), 1) < 4
-    for parity, (one, two) in enumerate(((own, swapped), (swapped, own))):
-        for half in range(2):
-            lanes = half * 256
-            block = jnp.where(upper, one[:, :, lanes : lanes + 128], two[:, :, lanes + 128 : lanes + 256])
-            send1[:, parity, half * 8 : (half + 1) * 8, :] = block.astype(BF16)
+    for q in range(4):
+        turned = dot_t(tab[2304:2560, 0:256], coded[q * 128 : (q + 1) * 128, :])
+        spread[pl.ds(q, 256, stride=4), :] = turned
+    send1[...] = spread[...].astype(BF16).reshape(2, rows // 2, 2, 8, 128)
 
     known_near()
-    for far, near in EARLY:
-        send_ring(send1, recv1, 0, far, near)
+    for c in range(2):
+        send_ring(send1.at[c], recv1.at[c], c, 8, 1)
     known_all()
-    for far, near in LATE:
-        send_ring(send1, recv1, 0, far, near)
-    send(send1, recv1, 0, 0, 1 - core)
-    keep_own(send1, recv1)
-    arrived(recv1, 0)
-
-    spread[...] = decode(recv1[...].reshape(rows * 16, 128).astype(F32))
-    parts = []
-    for part in range(2):
-        parts.append(
-            jnp.concatenate(
-                [
-                    spread[pl.ds(4 * q + 2 * part + c, rows, stride=16), :]
-                    for c in range(2)
-                    for q in range(4)
-                ],
-                axis=1,
-            )
-        )
-    hi, lo = halves(jnp.concatenate(parts, axis=0))
-    row_hi = tab[2304:2432, 256:384]
-    first = dot(row_hi, hi) + dot(row_hi, lo) + dot(tab[2432:2560, 256:384], hi)
+    for c in range(2):
+        send_ring(send1.at[c], recv1.at[c], c, 16, 9)
+        send(send1.at[c], recv1.at[c], c, 0, 1 - core)
+        keep_own(send1, recv1, c)
+
     twist = tab[2048:2176, :].astype(F32) + tab[2176:2304, :].astype(F32)
     tc = twist[:rows, :]
     ts = twist[rows:, :]
-    real, imag = [], []
-    for c in range(2):
-        re = first[:rows, c * 512 : (c + 1) * 512]
-        im = first[rows:, c * 512 : (c + 1) * 512]
-        real.append(tc * re + ts * im)
-        imag.append(tc * im - ts * re)
-    re_hi, re_lo = halves(jnp.concatenate(real, axis=0))
-    im_hi, im_lo = halves(jnp.concatenate(imag, axis=0))
-    res = dot_t(tab[0:512, :], re_hi) + dot_t(tab[0:512, :], re_lo) + dot_t(tab[512:1024, :], re_hi)
-    res = res + dot_t(tab[1024:1536, :], im_hi) + dot_t(tab[1024:1536, :], im_lo) + dot_t(tab[1536:2048, :], im_hi)
-    send2[...] = res.reshape(rows // 2, 2, 8, 128).astype(BF16)
-    send_ring(send2, recv2, 1, 16, 1)
-    send(send2, recv2, 1, 0, 1 - core)
-    keep_own(send2, recv2)
-    arrived(recv2, 1)
-
-    spread2[...] = recv2[...].astype(F32).reshape(rows * 8, 128)
-    low = lax.broadcasted_iota(jnp.int32, (rows, 128), 1) < 64
+    row_hi = tab[2304:2432, 256:384]
+    row_lo = tab[2432:2560, 256:384]
+    low = lax.broadcasted_iota(jnp.int32, (256, 128), 1) < 64
+    for c in range(2):
+        arrived(recv1.at[c], c)
+        base = c * 512
+        spread[base : base + 512, :] = decode(recv1[c].astype(F32).reshape(rows * 8, 128))
+        parts = []
+        for part in range(2):
+            parts.append(
+                jnp.concatenate(
+                    [spread[pl.ds(base + 4 * part + q, rows, stride=8), :] for q in range(4)], axis=1
+                )
+            )
+        hi, lo = halves(jnp.concatenate(parts, axis=0))
+        first = dot(row_hi, hi) + dot(row_hi, lo) + dot(row_lo, hi)
+        re = first[:rows, :]
+        im = first[rows:, :]
+        re_hi, re_lo = halves(tc * re + ts * im)
+        im_hi, im_lo = halves(tc * im - ts * re)
+        res = dot_t(tab[512:1024, :], jnp.concatenate([re_hi, re_hi], axis=0))
+        res = res + dot_t(tab[1536:2048, :], jnp.concatenate([im_hi, im_hi], axis=0))
+        both = dot_t(tab[0:512, :], jnp.concatenate([re_hi, re_hi, re_lo, re_lo], axis=0))
+        both = both + dot_t(tab[1024:1536, :], jnp.concatenate([im_hi, im_hi, im_lo, im_lo], axis=0))
+        spread2[...] = res + both[:, :128] + both[:, 128:]
+        paired = jnp.where(low, spread2[pl.ds(0, 256, stride=2), :], spread2[pl.ds(1, 256, stride=2), :])
+        send2[c] = paired.reshape(rows // 2, 2, 4, 128).astype(BF16)
+        send_ring(send2.at[c], recv2.at[c], 2 + c, 16, 1)
+        send(send2.at[c], recv2.at[c], 2 + c, 0, 1 - core)
+        keep_own(send2, recv2, c)
+
+    for c in range(2):
+        arrived(recv2.at[c], 2 + c)
+        spread2[c * 256 : (c + 1) * 256, :] = recv2[c].astype(F32).reshape(rows * 4, 128)
     for pair in range(4):
-        even = spread2[pl.ds(2 * pair, rows, stride=8), :]
-        odd = spread2[pl.ds(2 * pair + 1, rows, stride=8), :]
-        top = jnp.where(low, even, pltpu.roll(odd, 64, 1))
-        bottom = jnp.where(low, pltpu.roll(even, 64, 1), odd)
-        turned = jnp.concatenate([top, bottom], axis=0).T
+        turned = jnp.concatenate(
+            [spread2[pl.ds(c * 256 + pair, rows, stride=4), :] for c in range(2)], axis=0
+        ).T
         out_ref[pair * 128 : (pair + 1) * 128, :] = turned.astype(BF16)
-    departed(recv1, 0)
-    departed(recv2, 1)
+    for c in range(2):
+        departed(recv1.at[c], c)
+        departed(recv2.at[c], 2 + c)
 
 
 def body(tokens, out_weight):
@@ -261,14 +247,14 @@
     scratch += [
         pltpu.VMEM((2048, 512), BF16),
         pltpu.VMEM((rows * 16, 128), F32),
-        pltpu.VMEM((rows // 2, 2, 16, 128), BF16),
-        pltpu.VMEM((rows, 16, 128), BF16),
-        pltpu.VMEM((rows // 2, 2, 8, 128), BF16),
-        pltpu.VMEM((rows, 8, 128), BF16),
+        pltpu.VMEM((2, rows // 2, 2, 8, 128), BF16),
+        pltpu.VMEM((2, rows, 8, 128), BF16),
+        pltpu.VMEM((2, rows // 2, 2, 4, 128), BF16),
+        pltpu.VMEM((2, rows, 4, 128), BF16),
         pltpu.VMEM((rows * 8, 128), F32),
         pltpu.SemaphoreType.DMA((5,)),
-        pltpu.SemaphoreType.DMA((2,)),
-        pltpu.SemaphoreType.DMA((2,)),
+        pltpu.SemaphoreType.DMA((4,)),
+        pltpu.SemaphoreType.DMA((4,)),
         pltpu.SemaphoreType.REGULAR,
     ]
     return pl.pallas_call(

time: 71.7 us -> 68.9 us (0.961)
  Pallas kernels: 70.9 us -> 68.1 us
    pallas_call x1, Pallas kernels: 70.9 us -> 68.1 us  [body(): pl.pallas_call(functools.partial(kernel, rows), out_shape=jax.ShapeDtypeS...]
where the time goes in v2:
time: 68.9 us; the launch traced here: 68.8 us
  Pallas kernels  68.1 us (99%)
    pallas_call x1, Pallas kernels, body(): pl.pallas_call(functools.partial(kernel, rows), out_shape=jax.ShapeDtypeS...  68.1 us

profile of v2, /device:TPU:1, one launch (start us, length us, event | category | flops | bytes accessed | tf_op | source)
XLA Modules:
  0.0 68.8 jit_solution(3869936908106375706)
XLA Ops:
  0.0 68.1 %mix.1 = bf16[512,128]{1,0:T(8,128)(2,1)S(1)} custom-call(bf16[512,2048]{1,0:T(8,128)(2,1)} %x_hbm.1, bf16[2048,128]{1,0:T(8,128)(2,1)} %w_hbm.1, bf16[2560,512]{1,0:T(8,128)(2,1)} %constant.2.clone.tab_hbm), custom_call_target="tpu_custom_call" | custom-call | tf_op jit(solution)/shard_map/mix/pallas_call | solution.py:260
  68.1 0.7 copy.5

commit v3 on v2

--- a/solution.py
+++ b/solution.py
@@ -184,11 +184,13 @@
     send1[...] = spread[...].astype(BF16).reshape(2, rows // 2, 2, 8, 128)
 
     known_near()
-    for c in range(2):
-        send_ring(send1.at[c], recv1.at[c], c, 8, 1)
+    send_ring(send1.at[0], recv1.at[0], 0, 8, 1)
+    send_ring(send1.at[1], recv1.at[1], 1, 8, 5)
     known_all()
-    for c in range(2):
-        send_ring(send1.at[c], recv1.at[c], c, 16, 9)
+    send_ring(send1.at[0], recv1.at[0], 0, 16, 9)
+    send_ring(send1.at[1], recv1.at[1], 1, 16, 9)
+    send_ring(send1.at[1], recv1.at[1], 1, 4, 1)
+    for c in range(2):
         send(send1.at[c], recv1.at[c], c, 0, 1 - core)
         keep_own(send1, recv1, c)
 
@@ -200,6 +202,9 @@
     low = lax.broadcasted_iota(jnp.int32, (256, 128), 1) < 64
     for c in range(2):
         arrived(recv1.at[c], c)
+        if c == 1:
+            send_ring(send2.at[0], recv2.at[0], 2, 6, 1)
+            send(send2.at[0], recv2.at[0], 2, 0, 1 - core)
         base = c * 512
         spread[base : base + 512, :] = decode(recv1[c].astype(F32).reshape(rows * 8, 128))
         parts = []
@@ -222,10 +227,10 @@
         spread2[...] = res + both[:, :128] + both[:, 128:]
         paired = jnp.where(low, spread2[pl.ds(0, 256, stride=2), :], spread2[pl.ds(1, 256, stride=2), :])
         send2[c] = paired.reshape(rows // 2, 2, 4, 128).astype(BF16)
-        send_ring(send2.at[c], recv2.at[c], 2 + c, 16, 1)
-        send(send2.at[c], recv2.at[c], 2 + c, 0, 1 - core)
+        send_ring(send2.at[c], recv2.at[c], 2 + c, 16, 1 if c else 7)
         keep_own(send2, recv2, c)
 
+    send(send2.at[1], recv2.at[1], 3, 0, 1 - core)
     for c in range(2):
         arrived(recv2.at[c], 2 + c)
         spread2[c * 256 : (c + 1) * 256, :] = recv2[c].astype(F32).reshape(rows * 4, 128)

time: 68.9 us -> 67.7 us (0.983)
  Pallas kernels: 68.1 us -> 66.5 us
    pallas_call x1, Pallas kernels: 68.1 us -> 66.5 us  [body(): pl.pallas_call(functools.partial(kernel, rows), out_shape=jax.ShapeDtypeS...]
where the time goes in v3:
time: 67.7 us; the launch traced here: 67.2 us
  Pallas kernels  66.5 us (98%)
    pallas_call x1, Pallas kernels, body(): pl.pallas_call(functools.partial(kernel, rows), out_shape=jax.ShapeDtypeS...  66.5 us

profile of v3, /device:TPU:1, one launch (start us, length us, event | category | flops | bytes accessed | tf_op | source)
XLA Modules:
  0.0 67.2 jit_solution(7194239276184451077)
XLA Ops:
  0.0 66.5 %mix.1 = bf16[512,128]{1,0:T(8,128)(2,1)S(1)} custom-call(bf16[512,2048]{1,0:T(8,128)(2,1)} %x_hbm.1, bf16[2048,128]{1,0:T(8,128)(2,1)} %w_hbm.1, bf16[2560,512]{1,0:T(8,128)(2,1)} %constant.2.clone.tab_hbm), custom_call_target="tpu_custom_call" | custom-call | tf_op jit(solution)/shard_map/mix/pallas_call | solution.py:265
  66.5 0.7 copy.5

commit v4 on v3

--- a/solution.py
+++ b/solution.py
@@ -17,8 +17,8 @@
 
 FLOOR = 2.0**-6
 LIMIT = 34800.0
-SHIFT = 87.0
-GAIN = 175.0 / math.log1p(LIMIT / FLOOR)
+SHIFT = 125.0 * math.log(2.0)
+GAIN = (88.0 + SHIFT) / math.log1p(LIMIT / FLOOR)
 
 
 def split_table(table):
@@ -202,9 +202,6 @@
     low = lax.broadcasted_iota(jnp.int32, (256, 128), 1) < 64
     for c in range(2):
         arrived(recv1.at[c], c)
-        if c == 1:
-            send_ring(send2.at[0], recv2.at[0], 2, 6, 1)
-            send(send2.at[0], recv2.at[0], 2, 0, 1 - core)
         base = c * 512
         spread[base : base + 512, :] = decode(recv1[c].astype(F32).reshape(rows * 8, 128))
         parts = []
@@ -230,6 +227,8 @@
         send_ring(send2.at[c], recv2.at[c], 2 + c, 16, 1 if c else 7)
         keep_own(send2, recv2, c)
 
+    send_ring(send2.at[0], recv2.at[0], 2, 6, 1)
+    send(send2.at[0], recv2.at[0], 2, 0, 1 - core)
     send(send2.at[1], recv2.at[1], 3, 0, 1 - core)
     for c in range(2):
         arrived(recv2.at[c], 2 + c)

time: 67.7 us -> 66.9 us (0.988)
  no operation moved by 1% of the time
where the time goes in v4:
time: 66.9 us; the launch traced here: 66.8 us
  Pallas kernels  66.1 us (99%)
    pallas_call x1, Pallas kernels, body(): pl.pallas_call(functools.partial(kernel, rows), out_shape=jax.ShapeDtypeS...  66.1 us

profile of v4, /device:TPU:1, one launch (start us, length us, event | category | flops | bytes accessed | tf_op | source)
XLA Modules:
  0.0 66.8 jit_solution(11805260057415290150)
XLA Ops:
  0.0 66.1 %mix.1 = bf16[512,128]{1,0:T(8,128)(2,1)S(1)} custom-call(bf16[512,2048]{1,0:T(8,128)(2,1)} %x_hbm.1, bf16[2048,128]{1,0:T(8,128)(2,1)} %w_hbm.1, bf16[2560,512]{1,0:T(8,128)(2,1)} %constant.2.clone.tab_hbm), custom_call_target="tpu_custom_call" | custom-call | tf_op jit(solution)/shard_map/mix/pallas_call | solution.py:264
  66.1 0.7 copy.5

commit v5 on v4

--- a/solution.py
+++ b/solution.py
@@ -224,10 +224,10 @@
         spread2[...] = res + both[:, :128] + both[:, 128:]
         paired = jnp.where(low, spread2[pl.ds(0, 256, stride=2), :], spread2[pl.ds(1, 256, stride=2), :])
         send2[c] = paired.reshape(rows // 2, 2, 4, 128).astype(BF16)
-        send_ring(send2.at[c], recv2.at[c], 2 + c, 16, 1 if c else 7)
+        send_ring(send2.at[c], recv2.at[c], 2 + c, 16, 1 if c else 5)
         keep_own(send2, recv2, c)
 
-    send_ring(send2.at[0], recv2.at[0], 2, 6, 1)
+    send_ring(send2.at[0], recv2.at[0], 2, 4, 1)
     send(send2.at[0], recv2.at[0], 2, 0, 1 - core)
     send(send2.at[1], recv2.at[1], 3, 0, 1 - core)
     for c in range(2):

time: 66.9 us -> 67.2 us (level)
  no operation moved by 1% of the time
where the time goes in v5:
time: 67.2 us; the launch traced here: 66.8 us
  Pallas kernels  66.1 us (98%)
    pallas_call x1, Pallas kernels, body(): pl.pallas_call(functools.partial(kernel, rows), out_shape=jax.ShapeDtypeS...  66.1 us

profile of v5, /device:TPU:1, one launch (start us, length us, event | category | flops | bytes accessed | tf_op | source)
XLA Modules:
  0.0 66.8 jit_solution(14730390300580624339)
XLA Ops:
  0.0 66.1 %mix.1 = bf16[512,128]{1,0:T(8,128)(2,1)S(1)} custom-call(bf16[512,2048]{1,0:T(8,128)(2,1)} %x_hbm.1, bf16[2048,128]{1,0:T(8,128)(2,1)} %w_hbm.1, bf16[2560,512]{1,0:T(8,128)(2,1)} %constant.2.clone.tab_hbm), custom_call_target="tpu_custom_call" | custom-call | tf_op jit(solution)/shard_map/mix/pallas_call | solution.py:264
  66.1 0.7 copy.5
